TPU v7x, 32 devices: a whole 2x2x4 slice. The times are simulated.
32 devices in a mesh: grp: 2 (over y), fs: 4 (over z), tp: 4 (over x, core).
Axes of the slice: x: 2, y: 2, z: 4, core: 2. Of those that a mesh axis runs over, the one named last changes fastest.
Arguments:
- tokens: bfloat16 [8, 1024, 2048], P(('grp', 'fs'), None, 'tp'), parts along dimension 0, may hold values from -6 to 6
- mix_gain: float32 [2048], replicated, may hold values from 0.1 to 1.9
- in_matrix: float32 [2048, 1024], P('fs', 'tp'), may hold values from -0.125 to 0.125
- in_scale: float32 [1, 1024], P(None, 'tp'), may hold values from 0.5 to 2
- pool_mix: bfloat16 [8, 128, 128], P('tp'), may hold values from -0.5 to 0.5
- pool_scale: float32 [1, 1024], P(None, 'tp'), may hold values from 0.1 to 1.9
- out_matrix: float32 [1024, 2048], P('tp', 'fs'), may hold values from -0.25 to 0.25
- out_scale: float32 [1, 2048], P(None, 'fs'), may hold values from 0.5 to 2
- ffn_gain: float32 [2048], replicated, may hold values from 0.1 to 1.9
- gate_matrix: float32 [2048, 5632], P('fs', 'tp'), may hold values from -0.125 to 0.125
- gate_scale: float32 [1, 5632], P(None, 'tp'), may hold values from 0.5 to 2
- up_matrix: float32 [2048, 5632], P('fs', 'tp'), may hold values from -0.125 to 0.125
- up_scale: float32 [1, 5632], P(None, 'tp'), may hold values from 0.5 to 2
- gate_taps: float32 [3, 5632], P(None, 'tp'), may hold values from -4 to 4
- up_taps: float32 [3, 5632], P(None, 'tp'), may hold values from -4 to 4
- down_matrix: float32 [5632, 2048], P('tp', 'fs'), may hold values from -0.109375 to 0.109375
- down_scale: float32 [1, 2048], P(None, 'fs'), may hold values from 0.5 to 2
Outputs:
- layer_out: bfloat16 [8, 1024, 2048], P(('grp', 'fs'), None, 'tp'), parts along dimension 0
There are 2 independent parts, one for each index of `grp`. A program takes and returns all parts, laid end to end along the dimension named above; an argument that names none is the same for every part. Nothing has to cross between parts.
All inputs are finite; a program needn't handle non-finite values.
Results may differ from a plain program's by a relative error of at most 0.025.
Values may be sent and summed in bfloat16 or wider, within the bound.
No kernel may reach another device: no remote copies, remote signals or barrier semaphores. Data moves between devices by JAX's collectives and lax.ppermute only.
A program may use at most 128 MiB of HBM per device.

v0:
```python
import jax
import jax.numpy as jnp
from jax import lax
from jax.sharding import PartitionSpec as P

BLOCKS = 8
eps = 1e-06
widest_span = 16


def norm_rows(tok_rows, norm_gain):
    values = tok_rows.astype(jnp.float32)
    scaled = values * lax.rsqrt(jnp.mean(values * values, axis=-1, keepdims=True) + eps)
    return (scaled * norm_gain).astype(jnp.bfloat16)


def span_widths(block_ids):
    return jnp.left_shift(jnp.ones_like(block_ids), 1 + 4 * block_ids // BLOCKS)


def trailing_gap(projected, windows):
    values = projected.astype(jnp.float32)
    length = values.shape[0]
    running = values
    for offset in range(1, widest_span):
        shifted = jnp.pad(values[: length - offset], ((offset, 0), (0, 0)))
        running = running + jnp.where(windows[None, :] > offset, shifted, jnp.zeros_like(shifted))
    positions = jnp.arange(length, dtype=jnp.int32)[:, None]
    counts = jnp.minimum(positions + 1, windows[None, :]).astype(jnp.float32)
    return (running / counts - values).astype(jnp.bfloat16)


def causal_taps(linear, tap_table):
    values = linear.astype(jnp.float32)
    length = values.shape[0]
    back_one = jnp.pad(values[: length - 1], ((1, 0), (0, 0)))
    back_two = jnp.pad(values[: length - 2], ((2, 0), (0, 0)))
    return tap_table[2] * values + tap_table[1] * back_one + tap_table[0] * back_two


def fold_rows(operand, portion):
    return jnp.dot(operand, portion, preferred_element_type=jnp.float32)


def shards(
    tokens,
    mix_gain,
    in_matrix,
    in_scale,
    pool_mix,
    pool_scale,
    out_matrix,
    out_scale,
    ffn_gain,
    gate_matrix,
    gate_scale,
    up_matrix,
    up_scale,
    gate_taps,
    up_taps,
    down_matrix,
    down_scale,
):
    length = tokens.shape[1]
    own_width = tokens.shape[2]
    local_rows = tokens.reshape(length, own_width)
    gathered = lax.all_gather(local_rows, "tp", axis=1, tiled=True)
    normed = norm_rows(gathered, mix_gain)
    width_in = in_matrix.shape[1]
    in_total = fold_rows(
        normed, lax.all_gather(in_matrix.astype(jnp.bfloat16), "fs", axis=0, tiled=True)
    )
    projected = (in_total * in_scale).astype(jnp.bfloat16)
    local_blocks = pool_mix.shape[0]
    block_width = pool_mix.shape[1]
    block_ids = lax.axis_index("tp") * local_blocks + jnp.arange(local_blocks, dtype=jnp.int32)
    windows = jnp.repeat(span_widths(block_ids), block_width)
    spread = trailing_gap(projected, windows)
    block_mixed = jnp.einsum(
        "lbc,bce->lbe",
        spread.reshape(length, local_blocks, block_width),
        pool_mix,
        preferred_element_type=jnp.float32,
    ).reshape(length, width_in)
    pooled = (block_mixed * pool_scale).astype(jnp.bfloat16)
    out_cols = lax.all_gather(out_scale, "fs", axis=1, tiled=True)
    tp_index = lax.axis_index("tp")
    groups = lax.axis_size("tp")
    pooled_all = lax.all_gather(pooled, "tp", axis=1, tiled=True)
    row_block = lax.all_gather(out_matrix.astype(jnp.bfloat16), "fs", axis=1, tiled=True)
    own_matrix = lax.all_to_all(row_block, "tp", split_axis=1, concat_axis=0, tiled=True)
    own_scales = lax.dynamic_slice_in_dim(out_cols, tp_index * own_width, own_width, 1)
    grouped_rows = pooled_all.reshape(length, groups, width_in)
    grouped_matrix = own_matrix.reshape(groups, width_in, own_width)
    pieces = (
        jnp.einsum("lgc,gcd->gld", grouped_rows, grouped_matrix, preferred_element_type=jnp.float32)
        * own_scales[None]
    )
    rounded = lax.optimization_barrier(pieces.astype(jnp.bfloat16))
    mixing = jnp.sum(rounded.astype(jnp.float32), axis=0)
    residual = (local_rows.astype(jnp.float32) + mixing).astype(jnp.bfloat16)
    gathered_ffn = lax.all_gather(residual, "tp", axis=1, tiled=True)
    normed_ffn = norm_rows(gathered_ffn, ffn_gain)
    gate_cast = gate_matrix.astype(jnp.bfloat16)
    up_cast = up_matrix.astype(jnp.bfloat16)
    gate_full, up_full = (
        lax.all_gather(gate_cast, "fs", axis=0, tiled=True),
        lax.all_gather(up_cast, "fs", axis=0, tiled=True),
    )
    gate_total = jnp.dot(normed_ffn, gate_full, preferred_element_type=jnp.float32)
    up_total = jnp.dot(normed_ffn, up_full, preferred_element_type=jnp.float32)
    gate_lin = (gate_total * gate_scale).astype(jnp.bfloat16)
    up_lin = (up_total * up_scale).astype(jnp.bfloat16)
    hidden = (jax.nn.silu(causal_taps(gate_lin, gate_taps)) * causal_taps(up_lin, up_taps)).astype(
        jnp.bfloat16
    )
    down_cols = lax.all_gather(down_scale, "fs", axis=1, tiled=True)
    partial_ffn = (
        jnp.dot(
            hidden,
            lax.all_gather(down_matrix.astype(jnp.bfloat16), "fs", axis=1, tiled=True),
            preferred_element_type=jnp.float32,
        )
        * down_cols
    )
    feed_out = lax.psum_scatter(
        partial_ffn.astype(jnp.bfloat16), "tp", scatter_dimension=1, tiled=True
    ).astype(jnp.float32)
    result = (residual.astype(jnp.float32) + feed_out).astype(jnp.bfloat16)
    return result.reshape(1, length, result.shape[1])


def solution(mesh):
    return jax.shard_map(
        shards,
        mesh=mesh,
        in_specs=(
            P(("grp", "fs"), None, "tp"),
            P(),
            P("fs", "tp"),
            P(None, "tp"),
            P("tp", None, None),
            P(None, "tp"),
            P("tp", "fs"),
            P(None, "fs"),
            P(),
            P("fs", "tp"),
            P(None, "tp"),
            P("fs", "tp"),
            P(None, "tp"),
            P(None, "tp"),
            P(None, "tp"),
            P("tp", "fs"),
            P(None, "fs"),
        ),
        out_specs=P(("grp", "fs"), None, "tp"),
        check_vma=False,
    )
```

profile of v0, /device:TPU:0, one launch (start us, length us, event | category | flops | bytes accessed | tf_op | source)
XLA Modules:
  0.0 573.4 jit_solution(17679194408588764987)
XLA Ops:
  6.5 0.7 all-gather.24.cloned.1.call-update
  7.3 1.8 convert_element_type.120
  9.2 1.9 copy.22
  11.3 34.8 %all-gather.24.cloned.1.call-done = bf16[1,1024,2048]{2,1,0:T(8,128)(2,1)} async-done(((bf16[1,1024,512]{2,1,0:T(8,128)(2,1)}), bf16[1,1024,2048]{2,1,0:T(8,128)(2,1)}) %all-gather.24.cloned.1.call-update) | async-done | bytes 4194320 | tf_op jit(solution)/shard_map/all_gather | solution.py:67
  46.1 3.1 fusion.3
  49.2 26.5 %all-gather.10.cloned.1.call-done = bf16[2048,256]{1,0:T(8,128)(2,1)} async-done(((bf16[512,256]{1,0:T(8,128)(2,1)}), bf16[2048,256]{1,0:T(8,128)(2,1)}) %all-gather.10.cloned.1.call-update) | async-done | bytes 1048592 | tf_op jit(solution)/shard_map/all_gather | solution.py:71
  75.7 3.8 fusion.20
  80.1 3.2 fusion.28
  83.4 0.9 fusion.26
  84.3 20.3 %all-gather.14.cloned.1.call-done = bf16[256,2048]{0,1:T(8,128)(2,1)} async-done(((bf16[256,512]{0,1:T(8,128)(2,1)}), bf16[256,2048]{0,1:T(8,128)(2,1)}) %all-gather.14.cloned.1.call-update) | async-done | bytes 1048592 | tf_op jit(solution)/shard_map/all_gather | solution.py:90
  104.7 2.3 copy.23
  106.9 3.5 all-to-all-start
  110.5 11.9 %all_gather.34 = f32[1,2048]{1,0:T(1,128)S(1)} all-gather(f32[1,512]{1,0:T(1,128)S(1)} %copy-done.10), channel_id=1, replica_groups=mesh['grp'=2,'fs'=4,'tp'=4] {'fs'}, dimensions={1}, use_global_device_ids=true | all-gather | bytes 10240 | tf_op jit(solution)/shard_map/all_gather | solution.py:86
  122.5 12.5 %all-to-all-done = bf16[256,4,512]{2,0,1:T(8,128)(2,1)S(1)} async-done(((bf16[256,4,512]{2,0,1:T(8,128)(2,1)}), bf16[256,4,512]{2,0,1:T(8,128)(2,1)S(1)}, u32[]{:S(2)}, u32[]{:S(2)}) %all-to-all-start) | async-done | bytes 1048608 | tf_op jit(solution)/shard_map/all_to_all | solution.py:91
  135.0 2.7 all-gather.12.cloned.1.call-done
  137.6 3.0 multiply_convert_fusion.1
  140.6 0.7 convert_reduce_fusion
  141.3 1.3 fusion.13
  142.7 1.3 convert_element_type.133
  144.2 3.3 convert_element_type.136
  147.5 1.3 convert_element_type.140
  149.0 12.1 %all_gather.39 = f32[1,2048]{1,0:T(1,128)S(1)} all-gather(f32[1,512]{1,0:T(1,128)S(1)} %copy-done.11), channel_id=1, replica_groups=mesh['grp'=2,'fs'=4,'tp'=4] {'fs'}, dimensions={1}, use_global_device_ids=true | all-gather | bytes 10240 | tf_op jit(solution)/shard_map/all_gather | solution.py:117
  161.2 14.5 %all-gather.16.cloned.1.call-done = bf16[1024,2048]{1,0:T(8,128)(2,1)} async-done(((bf16[1024,512]{1,0:T(8,128)(2,1)}), bf16[1024,2048]{1,0:T(8,128)(2,1)}) %all-gather.16.cloned.1.call-update) | async-done | bytes 4194320 | tf_op jit(solution)/shard_map/all_gather | solution.py:102
  175.7 3.1 fusion
  178.8 105.1 %all-gather.18.cloned.1.call-done = bf16[2048,1408]{1,0:T(8,128)(2,1)} async-done(((bf16[512,1408]{1,0:T(8,128)(2,1)}), bf16[2048,1408]{1,0:T(8,128)(2,1)}) %all-gather.18.cloned.1.call-update) | async-done | bytes 5767184 | tf_op jit(solution)/shard_map/all_gather | solution.py:107
  283.9 11.9 %fusion.11 = f32[1024,1408]{1,0:T(8,128)} fusion(bf16[2048,1408]{1,0:T(8,128)(2,1)} %all-gather.18.cloned.1.call-done, f32[1408]{0:T(1024)S(1)} %reduce.1, bf16[1024,2048]{1,0:T(8,128)(2,1)} %all-gather.16.cloned.1.call-done, f32[2048]{0:T(1024)S(1)} %copy-done.14, f32[1024]{0:T(1024)S(1)} %add_rsqrt_fusion), kind=kOutput, calls=%fused_computation.20 | convolution fusion | flops 5918294016 | bytes 15746560 | tf_op jit(solution)/shard_map/dot_general | solution.py:110
  295.8 94.7 %all-gather.20.cloned.1.call-done = bf16[2048,1408]{1,0:T(8,128)(2,1)} async-done(((bf16[512,1408]{1,0:T(8,128)(2,1)}), bf16[2048,1408]{1,0:T(8,128)(2,1)}) %all-gather.20.cloned.1.call-update) | async-done | bytes 5767184 | tf_op jit(solution)/shard_map/all_gather | solution.py:108
  390.4 12.0 %fusion.12 = f32[1024,1408]{1,0:T(8,128)} fusion(bf16[2048,1408]{1,0:T(8,128)(2,1)} %all-gather.20.cloned.1.call-done, f32[1408]{0:T(1024)S(1)} %reduce.5, bf16[1024,2048]{1,0:T(8,128)(2,1)} %all-gather.16.cloned.1.call-done, f32[2048]{0:T(1024)S(1)} %copy-done.14, f32[1024]{0:T(1024)S(1)} %add_rsqrt_fusion), kind=kOutput, calls=%fused_computation.21 | convolution fusion | flops 5918294016 | bytes 15746560 | tf_op jit(solution)/shard_map/dot_general | solution.py:111
  402.4 94.6 %all-gather.22.cloned.1.call-done = bf16[1408,2048]{1,0:T(8,128)(2,1)} async-done(((bf16[1408,512]{1,0:T(8,128)(2,1)}), bf16[1408,2048]{1,0:T(8,128)(2,1)}) %all-gather.22.cloned.1.call-update) | async-done | bytes 5767184 | tf_op jit(solution)/shard_map/all_gather | solution.py:121
  497.0 24.6 %multiply_convert_fusion = bf16[1024,2048]{1,0:T(8,128)(2,1)} fusion(bf16[1408,2048]{1,0:T(8,128)(2,1)} %all-gather.22.cloned.1.call-done, f32[2048]{0:T(1024)S(1)} %bitcast.83, f32[1022,1408]{1,0:T(8,128)} %bitcast.89, f32[1023,1408]{1,0:T(8,128)} %bitcast.90, f32[1024,1408]{1,0:T(8,128)} %fusion.12, f32[1022,1408]{1,0:T(8,128)} %bitcast.87, ...), kind=kOutput, calls=%fused_computation.10 | convolution fusion | flops 5932843008 | bytes 44572672 | tf_op jit(solution)/shard_map/dot_general | solution.py:119
  521.6 42.8 %reduce-scatter.2.cloned.1.call-done = bf16[1024,512]{1,0:T(8,128)(2,1)} async-done(((bf16[1024,2048]{1,0:T(8,128)(2,1)}), bf16[1024,512]{1,0:T(8,128)(2,1)}) %reduce-scatter.2.cloned.1.call-update) | async-done | bytes 1048592 | tf_op jit(solution)/shard_map/reduce_scatter | solution.py:126
  564.4 2.5 fusion.25
  (67 shorter events, 1.4 us)
Async XLA Ops:
  6.5 73.6 %copy-start = (bf16[2,128,128]{2,1,0:T(8,128)(2,1)S(1)}, bf16[2,128,128]{2,1,0:T(8,128)(2,1)}, u32[]{:S(2)}) copy-start(bf16[2,128,128]{2,1,0:T(8,128)(2,1)} %param.21) | copy-start | bytes 196612
  6.5 69.2 %copy-start.15 = (f32[1,256]{1,0:T(1,128)S(1)}, f32[1,256]{1,0:T(1,128)}, u32[]{:S(2)}) copy-start(f32[1,256]{1,0:T(1,128)} %param.20) | copy-start | bytes 3076
  6.5 69.2 %copy-start.13 = (f32[2048]{0:T(1024)S(1)}, f32[2048]{0:T(1024)}, u32[]{:S(2)}) copy-start(f32[2048]{0:T(1024)} %param.18) | copy-start | bytes 24580
  6.5 39.6 %all-gather.24.cloned.1.call-start = ((), (), s32[]{:S(2)}) async-start(), calls=%async_computation.10 | async-start | bytes 5242880 | tf_op jit(solution)/shard_map/all_gather | solution.py:67
  7.3 68.4 %all-gather.10.cloned.1.call-start = ((), (), s32[]{:S(2)}) async-start(), calls=%async_computation.2 | async-start | bytes 1310720 | tf_op jit(solution)/shard_map/all_gather | solution.py:71
  9.1 95.6 %all-gather.14.cloned.1.call-start = ((), (), s32[]{:S(2)}) async-start(), calls=%async_computation.4 | async-start | bytes 1310720 | tf_op jit(solution)/shard_map/all_gather | solution.py:90
  11.1 126.6 %all-gather.12.cloned.1.call-start = ((), (), s32[]{:S(2)}) async-start(), calls=%async_computation.3 | async-start | bytes 2621440 | tf_op jit(solution)/shard_map/all_gather | solution.py:89
  80.1 3.3 copy-start.12
  83.4 27.1 %copy-start.10 = (f32[1,512]{1,0:T(1,128)S(1)}, f32[1,512]{1,0:T(1,128)}, u32[]{:S(2)}) copy-start(f32[1,512]{1,0:T(1,128)} %param.24) | copy-start | bytes 6148
  106.9 28.0 %all-to-all-start = ((bf16[256,4,512]{2,0,1:T(8,128)(2,1)}), bf16[256,4,512]{2,0,1:T(8,128)(2,1)S(1)}, u32[]{:S(2)}, u32[]{:S(2)}) async-start(bf16[256,4,512]{2,0,1:T(8,128)(2,1)} %copy.23), calls=%async_computation | async-start | bytes 2097152 | tf_op jit(solution)/shard_map/all_to_all | solution.py:91
  110.5 65.3 %all-gather.16.cloned.1.call-start = ((), (), s32[]{:S(2)}) async-start(), calls=%async_computation.5 | async-start | bytes 5242880 | tf_op jit(solution)/shard_map/all_gather | solution.py:102
  137.6 3.7 copy-start.3
  140.6 2.1 copy-start.4
  142.7 141.2 %all-gather.18.cloned.1.call-start = ((), (), s32[]{:S(2)}) async-start(), calls=%async_computation.6 | async-start | bytes 7208960 | tf_op jit(solution)/shard_map/all_gather | solution.py:107
  144.0 3.5 copy-start.5
  144.1 4.8 copy-start.8
  144.1 4.9 copy-start.9
  144.1 4.9 copy-start.11
  144.1 17.0 %copy-start.6 = (f32[3,1408]{1,0:T(4,128)S(1)}, f32[3,1408]{1,0:T(4,128)}, u32[]{:S(2)}) copy-start(f32[3,1408]{1,0:T(4,128)} %param.31) | copy-start | bytes 50692
  144.1 17.0 %copy-start.7 = (f32[3,1408]{1,0:T(4,128)S(1)}, f32[3,1408]{1,0:T(4,128)}, u32[]{:S(2)}) copy-start(f32[3,1408]{1,0:T(4,128)} %param.30) | copy-start | bytes 50692
  144.1 246.3 %all-gather.20.cloned.1.call-start = ((), (), s32[]{:S(2)}) async-start(), calls=%async_computation.7 | async-start | bytes 7208960 | tf_op jit(solution)/shard_map/all_gather | solution.py:108
  147.5 136.4 %copy-start.14 = (f32[2048]{0:T(1024)S(1)}, f32[2048]{0:T(1024)}, u32[]{:S(2)}) copy-start(f32[2048]{0:T(1024)} %param.25) | copy-start | bytes 24580
  147.5 349.5 %all-gather.22.cloned.1.call-start = ((), (), s32[]{:S(2)}) async-start(), calls=%async_computation.8 | async-start | bytes 7208960 | tf_op jit(solution)/shard_map/all_gather | solution.py:121
  148.8 415.6 %reduce-scatter.2.cloned.1.call-start = ((), (), s32[]{:S(2)}) async-start(), calls=%async_computation.9 | async-start | bytes 5242880 | tf_op jit(solution)/shard_map/reduce_scatter | solution.py:126
  497.0 67.4 %copy-start.2 = (bf16[1024,512]{1,0:T(8,128)(2,1)S(1)}, bf16[1024,512]{1,0:T(8,128)(2,1)}, u32[]{:S(2)}) copy-start(bf16[1024,512]{1,0:T(8,128)(2,1)} %fusion.13) | copy-start | bytes 3145732
  497.0 69.9 %copy-start.1 = (bf16[2,128,128]{2,1,0:T(8,128)(2,1)S(1)}, bf16[2,128,128]{2,1,0:T(8,128)(2,1)}, u32[]{:S(2)}) copy-start(bf16[2,128,128]{2,1,0:T(8,128)(2,1)} %param.21) | copy-start | bytes 196612
Sparse Core Ops, SparseCore 0:
  8.9 37.1 all-gather.23
  47.7 27.9 all-gather.9
  77.3 27.3 all-gather.13
  106.1 31.4 all-gather.11
  142.8 32.9 all-gather.15
  177.2 106.6 all-gather.17
  285.5 104.9 all-gather.19
  392.0 104.9 all-gather.21
  521.8 42.6 reduce-scatter.1
where the time goes:
time: 574 us; the launch traced here: 573 us
  waiting for transfers between devices  449 us (78%)
  matrix products  58.5 us (10%)
  blocking collectives  24.1 us (4%)
  other arithmetic  19.3 us (3%)
  between operations  13.5 us (2%)
    all_gather x1, waiting for transfers between devices, shards(): lax.all_gather(gate_cast, 'fs', axis=0, tiled=True)  105 us
    all_gather x1, waiting for transfers between devices, shards(): lax.all_gather(up_cast, 'fs', axis=0, tiled=True)  94.7 us
    all_gather x1, waiting for transfers between devices, shards(): lax.all_gather(down_matrix.astype(jnp.bfloat16), 'fs', axis=1, tiled=True)  94.6 us
    reduce_scatter x1, waiting for transfers between devices, shards(): lax.psum_scatter(partial_ffn.astype(jnp.bfloat16), 'tp', scatter_dimensio...  42.8 us
    all_gather x1, waiting for transfers between devices, shards(): gathered = lax.all_gather(local_rows, 'tp', axis=1, tiled=True)  34.8 us
    all_gather x1, waiting for transfers between devices, shards(): lax.all_gather(in_matrix.astype(jnp.bfloat16), 'fs', axis=0, tiled=True)  26.5 us
    dot_general x1, matrix products, shards(): jnp.dot(hidden, lax.all_gather(down_matrix.astype(jnp.bfloat16), 'fs', ax...  24.6 us
    all_gather x1, waiting for transfers between devices, shards(): lax.all_gather(out_matrix.astype(jnp.bfloat16), 'fs', axis=1, tiled=True)  20.3 us
  transfers between devices with their start and end apart: 10, of which 10 were waited for; matrix products, arithmetic and copies ran while one was open for 9% of the time, Pallas kernels for 0%

commit v1 on v0

--- a/solution.py
+++ b/solution.py
@@ -6,6 +6,18 @@
 BLOCKS = 8
 eps = 1e-06
 widest_span = 16
+
+
+def doubled_up(x, axis, dim):
+    ways, here = (lax.axis_size(axis), lax.axis_index(axis))
+    grown, reach = (x, 1)
+    while reach < ways:
+        theirs = lax.ppermute(grown, axis, [(d, d ^ reach) for d in range(ways)])
+        mine_first = jnp.concatenate([grown, theirs], axis=dim)
+        theirs_first = jnp.concatenate([theirs, grown], axis=dim)
+        grown = jnp.where(here & reach == 0, mine_first, theirs_first)
+        reach = 2 * reach
+    return grown
 
 
 def norm_rows(tok_rows, norm_gain):
@@ -118,7 +130,7 @@
     partial_ffn = (
         jnp.dot(
             hidden,
-            lax.all_gather(down_matrix.astype(jnp.bfloat16), "fs", axis=1, tiled=True),
+            doubled_up(down_matrix.astype(jnp.bfloat16), "fs", 1),
             preferred_element_type=jnp.float32,
         )
         * down_cols

time: 574 us -> 594 us (1.035)
  blocking collectives: 24.1 us -> 51.5 us
  waiting for transfers between devices: 449 us -> 432 us
    all_gather x1 -> x0, waiting for transfers between devices: 94.6 us -> none  [shards(): lax.all_gather(down_matrix.astype(jnp.bfloat16), 'fs', axis=1, tiled=True)]
    all_gather x1, waiting for transfers between devices: 105 us -> 194 us  [shards(): lax.all_gather(gate_cast, 'fs', axis=0, tiled=True)]
    all_gather x1, blocking collectives: 12.1 us -> 39.5 us  [shards(): down_cols = lax.all_gather(down_scale, 'fs', axis=1, tiled=True)]
    all_gather x1, waiting for transfers between devices: 14.5 us -> 0.01 us  [shards(): gathered_ffn = lax.all_gather(residual, 'tp', axis=1, tiled=True)]
  transfers between devices with their start and end apart: 10 -> 11, of which waited for: 10 -> 8; matrix products, arithmetic and copies ran while one was open for 9% -> 9% of each run, Pallas kernels for 0% -> 0%
where the time goes in v1:
time: 594 us; the launch traced here: 593 us
  waiting for transfers between devices  432 us (73%)
  matrix products  61.4 us (10%)
  blocking collectives  51.5 us (9%)
  other arithmetic  22.3 us (4%)
  between operations  13.8 us (2%)
  local copies, waits for them, and re-layouts  6.49 us (1%)
  starting transfers between devices  6.19 us (1%)
    all_gather x1, waiting for transfers between devices, shards(): lax.all_gather(gate_cast, 'fs', axis=0, tiled=True)  194 us
    all_gather x1, waiting for transfers between devices, shards(): lax.all_gather(up_cast, 'fs', axis=0, tiled=True)  97.5 us
    reduce_scatter x1, waiting for transfers between devices, shards(): lax.psum_scatter(partial_ffn.astype(jnp.bfloat16), 'tp', scatter_dimensio...  42.7 us
    all_gather x1, blocking collectives, shards(): down_cols = lax.all_gather(down_scale, 'fs', axis=1, tiled=True)  39.5 us
    all_gather x1, waiting for transfers between devices, shards(): gathered = lax.all_gather(local_rows, 'tp', axis=1, tiled=True)  34.8 us
    dot_general x1, matrix products, shards(): jnp.dot(hidden, doubled_up(down_matrix.astype(jnp.bfloat16), 'fs', 1), pr...  27.6 us
    all_gather x1, waiting for transfers between devices, shards(): lax.all_gather(in_matrix.astype(jnp.bfloat16), 'fs', axis=0, tiled=True)  26.5 us
    all_gather x1, waiting for transfers between devices, shards(): lax.all_gather(out_matrix.astype(jnp.bfloat16), 'fs', axis=1, tiled=True)  20.3 us
  transfers between devices with their start and end apart: 11, of which 8 were waited for; matrix products, arithmetic and copies ran while one was open for 9% of the time, Pallas kernels for 0%

profile of v1, /device:TPU:0, one launch (start us, length us, event | category | flops | bytes accessed | tf_op | source)
XLA Modules:
  0.0 593.3 jit_solution(5893123763095650738)
XLA Ops:
  7.3 1.8 convert_element_type.120
  9.2 1.9 copy.22
  11.3 34.8 %all-gather.21.cloned.1.call-done = bf16[1,1024,2048]{2,1,0:T(8,128)(2,1)} async-done(((bf16[1,1024,512]{2,1,0:T(8,128)(2,1)}), bf16[1,1024,2048]{2,1,0:T(8,128)(2,1)}) %all-gather.21.cloned.1.call-update) | async-done | bytes 4194320 | tf_op jit(solution)/shard_map/all_gather | solution.py:79
  46.1 3.1 fusion.3
  49.2 26.5 %all-gather.9.cloned.1.call-done = bf16[2048,256]{1,0:T(8,128)(2,1)} async-done(((bf16[512,256]{1,0:T(8,128)(2,1)}), bf16[2048,256]{1,0:T(8,128)(2,1)}) %all-gather.9.cloned.1.call-update) | async-done | bytes 1048592 | tf_op jit(solution)/shard_map/all_gather | solution.py:83
  75.7 3.8 fusion.27
  80.1 3.2 fusion.35
  83.4 0.9 fusion.33
  84.3 20.3 %all-gather.13.cloned.1.call-done = bf16[256,2048]{0,1:T(8,128)(2,1)} async-done(((bf16[256,512]{0,1:T(8,128)(2,1)}), bf16[256,2048]{0,1:T(8,128)(2,1)}) %all-gather.13.cloned.1.call-update) | async-done | bytes 1048592 | tf_op jit(solution)/shard_map/all_gather | solution.py:102
  104.7 2.3 copy.23
  106.9 3.5 all-to-all-start
  110.5 11.9 %all_gather.31 = f32[1,2048]{1,0:T(1,128)S(1)} all-gather(f32[1,512]{1,0:T(1,128)S(1)} %copy-done.9), channel_id=1, replica_groups=mesh['grp'=2,'fs'=4,'tp'=4] {'fs'}, dimensions={1}, use_global_device_ids=true | all-gather | bytes 10240 | tf_op jit(solution)/shard_map/all_gather | solution.py:98
  122.5 12.5 %all-to-all-done = bf16[256,4,512]{2,0,1:T(8,128)(2,1)S(1)} async-done(((bf16[256,4,512]{2,0,1:T(8,128)(2,1)}), bf16[256,4,512]{2,0,1:T(8,128)(2,1)S(1)}, u32[]{:S(2)}, u32[]{:S(2)}) %all-to-all-start) | async-done | bytes 1048608 | tf_op jit(solution)/shard_map/all_to_all | solution.py:103
  135.0 2.7 all-gather.11.cloned.1.call-done
  137.6 3.0 multiply_convert_fusion.1
  141.3 1.3 fusion.20
  142.7 1.3 convert_element_type.133
  144.1 3.2 convert_element_type.136
  147.3 2.3 convert_element_type.140
  149.7 1.5 collective-permute-start
  151.2 39.5 %all_gather.35 = f32[1,2048]{1,0:T(1,128)S(1)} all-gather(f32[1,512]{1,0:T(1,128)S(1)} %copy-done.10), channel_id=1, replica_groups=mesh['grp'=2,'fs'=4,'tp'=4] {'fs'}, dimensions={1}, use_global_device_ids=true | all-gather | bytes 10240 | tf_op jit(solution)/shard_map/all_gather | solution.py:129
  190.9 2.0 maximum_select_fusion.4
  192.9 0.9 collective-permute-start.1
  193.8 3.1 fusion
  196.9 193.8 %all-gather.17.cloned.1.call-done = bf16[2048,1408]{1,0:T(8,128)(2,1)} async-done(((bf16[512,1408]{1,0:T(8,128)(2,1)}), bf16[2048,1408]{1,0:T(8,128)(2,1)}) %all-gather.17.cloned.1.call-update) | async-done | bytes 5767184 | tf_op jit(solution)/shard_map/all_gather | solution.py:119
  390.8 12.0 %fusion.18 = f32[1024,1408]{1,0:T(8,128)} fusion(bf16[2048,1408]{1,0:T(8,128)(2,1)} %all-gather.17.cloned.1.call-done, f32[1408]{0:T(1024)S(1)} %reduce.1, bf16[1024,2048]{1,0:T(8,128)(2,1)} %all-gather.15.cloned.1.call-done, f32[2048]{0:T(1024)S(1)} %copy-done.14, f32[1024]{0:T(1024)S(1)} %add_rsqrt_fusion), kind=kOutput, calls=%fused_computation.28 | convolution fusion | flops 5918294016 | bytes 15746560 | tf_op jit(solution)/shard_map/dot_general | solution.py:122
  402.8 97.5 %all-gather.19.cloned.1.call-done = bf16[2048,1408]{1,0:T(8,128)(2,1)} async-done(((bf16[512,1408]{1,0:T(8,128)(2,1)}), bf16[2048,1408]{1,0:T(8,128)(2,1)}) %all-gather.19.cloned.1.call-update) | async-done | bytes 5767184 | tf_op jit(solution)/shard_map/all_gather | solution.py:120
  500.2 11.9 %fusion.19 = f32[1024,1408]{1,0:T(8,128)} fusion(bf16[2048,1408]{1,0:T(8,128)(2,1)} %all-gather.19.cloned.1.call-done, f32[1408]{0:T(1024)S(1)} %reduce.5, bf16[1024,2048]{1,0:T(8,128)(2,1)} %all-gather.15.cloned.1.call-done, f32[2048]{0:T(1024)S(1)} %copy-done.14, f32[1024]{0:T(1024)S(1)} %add_rsqrt_fusion), kind=kOutput, calls=%fused_computation.29 | convolution fusion | flops 5918294016 | bytes 15746560 | tf_op jit(solution)/shard_map/dot_general | solution.py:123
  512.1 1.5 copy-done.12
  513.7 27.6 %multiply_convert_fusion = bf16[1024,2048]{1,0:T(8,128)(2,1)} fusion(f32[2048]{0:T(1024)S(1)} %bitcast.82, bf16[1408,1024]{1,0:T(8,128)(2,1)} %copy-done.12, bf16[1408,1024]{1,0:T(8,128)(2,1)} %maximum_select_fusion.4, pred[]{:T(512)S(6)} %eq.6, f32[1022,1408]{1,0:T(8,128)} %bitcast.88, f32[1023,1408]{1,0:T(8,128)} %bitcast.89, f32[1024,1408]{1,0:T(8,128)} %fusion.19, ...), kind=kOutput, calls=%fused_computation.10 | convolution fusion | flops 5958795264 | bytes 44572672 | tf_op jit(solution)/shard_map/dot_general | solution.py:131
  541.2 42.7 %reduce-scatter.2.cloned.1.call-done = bf16[1024,512]{1,0:T(8,128)(2,1)} async-done(((bf16[1024,2048]{1,0:T(8,128)(2,1)}), bf16[1024,512]{1,0:T(8,128)(2,1)}) %reduce-scatter.2.cloned.1.call-update) | async-done | bytes 1048592 | tf_op jit(solution)/shard_map/reduce_scatter | solution.py:138
  583.9 2.5 fusion.32
  (69 shorter events, 2.7 us)
Async XLA Ops:
  6.5 73.6 %copy-start = (bf16[2,128,128]{2,1,0:T(8,128)(2,1)S(1)}, bf16[2,128,128]{2,1,0:T(8,128)(2,1)}, u32[]{:S(2)}) copy-start(bf16[2,128,128]{2,1,0:T(8,128)(2,1)} %param.21) | copy-start | bytes 196612
  6.5 69.2 %copy-start.15 = (f32[1,256]{1,0:T(1,128)S(1)}, f32[1,256]{1,0:T(1,128)}, u32[]{:S(2)}) copy-start(f32[1,256]{1,0:T(1,128)} %param.20) | copy-start | bytes 3076
  6.5 69.2 %copy-start.13 = (f32[2048]{0:T(1024)S(1)}, f32[2048]{0:T(1024)}, u32[]{:S(2)}) copy-start(f32[2048]{0:T(1024)} %param.18) | copy-start | bytes 24580
  6.5 39.6 %all-gather.21.cloned.1.call-start = ((), (), s32[]{:S(2)}) async-start(), calls=%async_computation.9 | async-start | bytes 5242880 | tf_op jit(solution)/shard_map/all_gather | solution.py:79
  7.3 68.4 %all-gather.9.cloned.1.call-start = ((), (), s32[]{:S(2)}) async-start(), calls=%async_computation.2 | async-start | bytes 1310720 | tf_op jit(solution)/shard_map/all_gather | solution.py:83
  9.1 95.6 %all-gather.13.cloned.1.call-start = ((), (), s32[]{:S(2)}) async-start(), calls=%async_computation.4 | async-start | bytes 1310720 | tf_op jit(solution)/shard_map/all_gather | solution.py:102
  11.1 126.6 %all-gather.11.cloned.1.call-start = ((), (), s32[]{:S(2)}) async-start(), calls=%async_computation.3 | async-start | bytes 2621440 | tf_op jit(solution)/shard_map/all_gather | solution.py:101
  80.1 3.3 copy-start.11
  83.4 27.1 %copy-start.9 = (f32[1,512]{1,0:T(1,128)S(1)}, f32[1,512]{1,0:T(1,128)}, u32[]{:S(2)}) copy-start(f32[1,512]{1,0:T(1,128)} %param.24) | copy-start | bytes 6148
  106.9 28.0 %all-to-all-start = ((bf16[256,4,512]{2,0,1:T(8,128)(2,1)}), bf16[256,4,512]{2,0,1:T(8,128)(2,1)S(1)}, u32[]{:S(2)}, u32[]{:S(2)}) async-start(bf16[256,4,512]{2,0,1:T(8,128)(2,1)} %copy.23), calls=%async_computation | async-start | bytes 2097152 | tf_op jit(solution)/shard_map/all_to_all | solution.py:103
  110.5 83.4 %all-gather.15.cloned.1.call-start = ((), (), s32[]{:S(2)}) async-start(), calls=%async_computation.5 | async-start | bytes 5242880 | tf_op jit(solution)/shard_map/all_gather | solution.py:114
  137.6 3.7 copy-start.3
  140.6 2.1 copy-start.4
  142.7 248.1 %all-gather.17.cloned.1.call-start = ((), (), s32[]{:S(2)}) async-start(), calls=%async_computation.6 | async-start | bytes 7208960 | tf_op jit(solution)/shard_map/all_gather | solution.py:119
  144.0 7.1 %copy-start.7 = (f32[1,1408]{1,0:T(1,128)S(1)}, f32[1,1408]{1,0:T(1,128)}, u32[]{:S(2)}) copy-start(f32[1,1408]{1,0:T(1,128)} %param.27) | copy-start | bytes 16900
  144.0 7.2 %copy-start.8 = (f32[1,1408]{1,0:T(1,128)S(1)}, f32[1,1408]{1,0:T(1,128)}, u32[]{:S(2)}) copy-start(f32[1,1408]{1,0:T(1,128)} %param.29) | copy-start | bytes 16900
  144.0 7.2 %copy-start.10 = (f32[1,512]{1,0:T(1,128)S(1)}, f32[1,512]{1,0:T(1,128)}, u32[]{:S(2)}) copy-start(f32[1,512]{1,0:T(1,128)} %param.33) | copy-start | bytes 6148
  144.0 46.7 %copy-start.5 = (f32[3,1408]{1,0:T(4,128)S(1)}, f32[3,1408]{1,0:T(4,128)}, u32[]{:S(2)}) copy-start(f32[3,1408]{1,0:T(4,128)} %param.31) | copy-start | bytes 50692
  144.0 46.7 %copy-start.6 = (f32[3,1408]{1,0:T(4,128)S(1)}, f32[3,1408]{1,0:T(4,128)}, u32[]{:S(2)}) copy-start(f32[3,1408]{1,0:T(4,128)} %param.30) | copy-start | bytes 50692
  144.0 356.2 %all-gather.19.cloned.1.call-start = ((), (), s32[]{:S(2)}) async-start(), calls=%async_computation.7 | async-start | bytes 7208960 | tf_op jit(solution)/shard_map/all_gather | solution.py:120
  147.3 436.7 %reduce-scatter.2.cloned.1.call-start = ((), (), s32[]{:S(2)}) async-start(), calls=%async_computation.8 | async-start | bytes 5242880 | tf_op jit(solution)/shard_map/reduce_scatter | solution.py:138
  149.7 241.1 %copy-start.14 = (f32[2048]{0:T(1024)S(1)}, f32[2048]{0:T(1024)}, u32[]{:S(2)}) copy-start(f32[2048]{0:T(1024)} %param.25) | copy-start | bytes 24580
  149.7 41.2 %collective-permute-start = (bf16[1408,512]{1,0:T(8,128)(2,1)S(1)}, bf16[1408,512]{1,0:T(8,128)(2,1)S(1)}, u32[]{:S(2)}, u32[]{:S(2)}) collective-permute-start(bf16[1408,512]{1,0:T(8,128)(2,1)S(1)} %convert_element_type.140), channel_id=1, source_target_pairs={{0,4},{4,0},{8,12},{12,8},{1,5},{5,1},{9,13},{13,9},{2,6},{6,2},{1... | collective-permute-start | bytes 4325384 | tf_op jit(solution)/shard_map/ppermute | solution.py:15
  192.9 319.2 %collective-permute-start.1 = (bf16[1408,1024]{1,0:T(8,128)(2,1)}, bf16[1408,1024]{1,0:T(8,128)(2,1)S(1)}, u32[]{:S(2)}, u32[]{:S(2)}) collective-permute-start(bf16[1408,1024]{1,0:T(8,128)(2,1)} %maximum_select_fusion.4), channel_id=1, source_target_pairs={{0,8},{4,12},{8,0},{12,4},{1,9},{5,13},{9,1},{13,5},{2,10},{6,14},... | collective-permute-start | bytes 8650760 | tf_op jit(solution)/shard_map/ppermute | solution.py:15
  512.1 1.5 copy-start.12
  513.7 70.3 %copy-start.2 = (bf16[1024,512]{1,0:T(8,128)(2,1)S(1)}, bf16[1024,512]{1,0:T(8,128)(2,1)}, u32[]{:S(2)}) copy-start(bf16[1024,512]{1,0:T(8,128)(2,1)} %fusion.20) | copy-start | bytes 3145732
  513.7 72.8 %copy-start.1 = (bf16[2,128,128]{2,1,0:T(8,128)(2,1)S(1)}, bf16[2,128,128]{2,1,0:T(8,128)(2,1)}, u32[]{:S(2)}) copy-start(bf16[2,128,128]{2,1,0:T(8,128)(2,1)} %param.21) | copy-start | bytes 196612
Sparse Core Ops, SparseCore 0:
  8.9 37.1 all-gather.20
  47.7 27.9 all-gather.8
  77.3 27.3 all-gather.12
  106.1 31.4 all-gather.10
  142.8 32.9 all-gather.14
  177.2 213.5 all-gather.16
  392.4 107.8 all-gather.18
  541.4 42.5 reduce-scatter.1
